TPU v7x, 32 devices: a whole 2x2x4 slice. The times are simulated.
32 devices in a mesh: grp: 2 (over y), ep: 16 (over z, x, core), tp: 1.
Axes of the slice: x: 2, y: 2, z: 4, core: 2. Of those that a mesh axis runs over, the one named last changes fastest.
Arguments:
- tokens: bfloat16 [2048, 2048], P(('grp', 'ep')), parts along dimension 0, may hold values from -6 to 6
- norm_gain: float32 [2048], replicated, may hold values from 0.1 to 1.9
- routes: int32 [2048, 6], P(('grp', 'ep')), parts along dimension 0, may hold values from 0 to 15, all different within a row; in each aligned block of 64 rows (0 to 63, 64 to 127, ...) at most 48 rows name the same one
- route_weights: float32 [2048, 6], P(('grp', 'ep')), parts along dimension 0, may hold values from 0.05 to 1
- w_gate: bfloat16 [16, 2048, 2048], P('ep', None, 'tp'), may hold values from -0.125 to 0.125
- w_up: bfloat16 [16, 2048, 2048], P('ep', None, 'tp'), may hold values from -0.125 to 0.125
- w_down: bfloat16 [16, 2048, 2048], P('ep', 'tp'), may hold values from -4 to 4
- final_gain: float32 [2048], P('tp'), may hold values from 0.1 to 1.9
Outputs:
- mixed_out: bfloat16 [2048, 2048], P(('grp', 'ep'), 'tp'), parts along dimension 0
There are 2 independent parts, one for each index of `grp`. A program takes and returns all parts, laid end to end along the dimension named above; an argument that names none is the same for every part. Nothing has to cross between parts.
Inputs may be any that keep to these rules, and one draw needn't show every extreme that they name: `routes`: each row names 6 different experts; within the rows of one index of ep no expert is named by more than 48 rows, and in every draw some expert is named by exactly 48 rows of some index.
All inputs are finite; a program needn't handle non-finite values.
Results may differ from a plain program's by a relative error of at most 0.015.
Values may be sent and summed in bfloat16 or wider, within the bound.
A program may use at most 64 MiB of HBM per device.

v0:
```python
import jax
import jax.numpy as jnp
from jax import lax
from jax.sharding import PartitionSpec as P

TOP_K = 6


EPS = 1e-06


def slot_table(route_rows, experts_all, capacity):
    flattened = route_rows.reshape(-1)
    matches = (flattened[:, None] == jnp.arange(experts_all, dtype=jnp.int32)[None, :]).astype(
        jnp.int32
    )
    earlier = jnp.cumsum(matches, axis=0) - matches
    slot_of = jnp.sum(earlier * matches, axis=1)
    return (flattened * capacity + slot_of).reshape(route_rows.shape)


def per_device(tokens, norm_gain, routes, route_weights, w_gate, w_up, w_down, final_gain):
    tok_count, features = tokens.shape
    ep_size = lax.axis_size("ep")
    exp_local = w_gate.shape[0]
    experts_all = exp_local * ep_size
    capacity = max(2, min(tok_count, 2 * tok_count * TOP_K // experts_all))
    slot_count = experts_all * capacity
    tokens_f = tokens.astype(jnp.float32)
    inverse = lax.rsqrt(jnp.mean(tokens_f * tokens_f, axis=1, keepdims=True) + EPS)
    normed = (tokens_f * inverse * norm_gain[None, :]).astype(jnp.bfloat16)
    places = slot_table(routes, experts_all, capacity)
    slot_ids = jnp.arange(slot_count, dtype=jnp.int32)
    matched = places[:, :, None] == slot_ids[None, None, :]
    selector = jnp.sum(matched.astype(jnp.float32), axis=1).T.astype(jnp.bfloat16)
    combine_rows = jnp.sum(jnp.where(matched, route_weights[:, :, None], 0.0), axis=1)
    outgoing = jnp.dot(selector, normed, preferred_element_type=jnp.float32).astype(jnp.bfloat16)
    outgoing = outgoing.reshape(ep_size, exp_local, capacity, features)
    received = lax.all_to_all(outgoing, "ep", split_axis=0, concat_axis=0, tiled=True)
    gate_value = jnp.einsum("secd,edf->secf", received, w_gate, preferred_element_type=jnp.float32)
    up_value = jnp.einsum("secd,edf->secf", received, w_up, preferred_element_type=jnp.float32)
    hidden = (jax.nn.silu(gate_value) * up_value).astype(jnp.bfloat16)
    partial_value = jnp.einsum("secf,efd->secd", hidden, w_down, preferred_element_type=jnp.float32)
    summed = lax.psum_scatter(
        partial_value.astype(jnp.bfloat16), "tp", scatter_dimension=3, tiled=True
    )
    returned = lax.all_to_all(summed, "ep", split_axis=0, concat_axis=0, tiled=True)
    results = returned.reshape(slot_count, returned.shape[3]).astype(jnp.float32)
    combined = jnp.dot(combine_rows, results, precision=lax.Precision.HIGHEST)
    local_squares = jnp.sum(combined * combined, axis=1)
    squares_all = lax.psum(local_squares, "tp")
    inverse_out = lax.rsqrt(squares_all / features + EPS)
    return (combined * inverse_out[:, None] * final_gain[None, :]).astype(jnp.bfloat16)


def solution(mesh):
    placed = (
        P(("grp", "ep"), None),
        P(),
        P(("grp", "ep"), None),
        P(("grp", "ep"), None),
        P("ep", None, "tp"),
        P("ep", None, "tp"),
        P("ep", "tp", None),
        P("tp"),
    )
    return jax.shard_map(
        per_device, mesh=mesh, in_specs=placed, out_specs=P(("grp", "ep"), "tp"), check_vma=False
    )
```

profile of v0, /device:TPU:0, one launch (start us, length us, event | category | flops | bytes accessed | tf_op | source)
XLA Modules:
  0.0 193.9 jit_solution(3700836418852448338)
XLA Ops:
  0.0 0.8 copy.33
  0.8 0.1 eq.42
  0.9 0.1 eq.38
  1.1 1.1 fusion.33
  2.2 0.9 reduce-window.6
  3.1 0.2 slice_reduce_fusion
  3.3 0.1 fusion.42
  3.4 0.1 reduce_sum.48
  3.6 0.1 copy.36
  3.6 0.0 copy-start.1
  3.6 0.9 multiply_add_fusion
  4.5 1.1 convert_reduce_fusion
  5.6 2.4 %convolution_convert_fusion = bf16[768,2048]{1,0:T(8,128)(2,1)S(1)} fusion(bf16[64,2048]{1,0:T(8,128)(2,1)} %param.8, f32[2048]{0:T(1024)} %param.9, f32[64]{0:T(128)S(1)} %add_rsqrt_fusion.1, bf16[64,768]{1,0:T(8,128)(2,1)S(1)} %get-tuple-element.5), kind=kOutput, calls=%fused_computation.14 | convolution fusion | flops 203423744 | bytes 3514624 | tf_op jit(solution)/shard_map/dot_general | solution.py:37
  8.0 76.8 %all_to_all.10 = bf16[16,1,48,2048]{3,2,1,0:T(8,128)(2,1)S(1)} all-to-all(bf16[16,1,48,2048]{3,2,1,0:T(8,128)(2,1)S(1)} %bitcast.110), channel_id=1, replica_groups=mesh['grp'=2,'ep'=16,'tp'=1] {'ep'}, dimensions={0} | all-to-all | bytes 6291456 | tf_op jit(solution)/shard_map/all_to_all | solution.py:39
  84.8 0.0 copy-done.1
  84.8 8.6 %fusion.4 = f32[16,48,2048]{2,1,0:T(8,128)} fusion(bf16[1,2048,2048]{2,1,0:T(8,128)(2,1)S(1)} %copy-done.1, bf16[16,1,48,2048]{3,2,1,0:T(8,128)(2,1)S(1)} %all_to_all.10), kind=kOutput, calls=%fused_computation.4 | convolution fusion | flops 6442450944 | bytes 17825792 | tf_op jit(solution)/shard_map/secd,edf->secf/dot_general | solution.py:40
  93.4 22.9 %fusion.24 = bf16[16,1,48,2048]{3,2,1,0:T(8,128)(2,1)} fusion(bf16[1,2048,2048]{2,1,0:T(8,128)(2,1)} %param.14, bf16[1,2048,2048]{2,1,0:T(8,128)(2,1)} %param.13, f32[16,48,2048]{2,1,0:T(8,128)} %fusion.4, bf16[16,1,48,2048]{3,2,1,0:T(8,128)(2,1)S(1)} %all_to_all.10), kind=kOutput, calls=%fused_computation.19 | convolution fusion | flops 12895911936 | bytes 29360128 | tf_op jit(solution)/shard_map/secf,efd->secd/dot_general | solution.py:43
  116.3 0.0 copy-start
  116.3 75.0 %all_to_all.11 = bf16[16,1,48,2048]{3,2,1,0:T(8,128)(2,1)S(1)} all-to-all(bf16[16,1,48,2048]{3,2,1,0:T(8,128)(2,1)} %fusion.24), channel_id=1, replica_groups=mesh['grp'=2,'ep'=16,'tp'=1] {'ep'}, dimensions={0} | all-to-all | bytes 6291456 | tf_op jit(solution)/shard_map/all_to_all | solution.py:47
  191.2 1.9 multiply_reduce_fusion
  193.1 0.0 copy-done
  193.1 0.8 multiply_convert_fusion
  (4 shorter events, 0.1 us)
Async XLA Ops:
  3.6 81.2 %copy-start.1 = (bf16[1,2048,2048]{2,1,0:T(8,128)(2,1)S(1)}, bf16[1,2048,2048]{2,1,0:T(8,128)(2,1)}, u32[]{:S(2)}) copy-start(bf16[1,2048,2048]{2,1,0:T(8,128)(2,1)} %param.12) | copy-start | bytes 25165828
  116.3 76.8 %copy-start = (f32[2048]{0:T(1024)S(1)}, f32[2048]{0:T(1024)}, u32[]{:S(2)}) copy-start(f32[2048]{0:T(1024)} %param.15) | copy-start | bytes 24580
where the time goes:
time: 195 us; the launch traced here: 194 us
  blocking collectives  152 us (78%)
  matrix products  35.7 us (18%)
  other arithmetic  4.93 us (3%)
    all_to_all x1, blocking collectives, per_device(): lax.all_to_all(outgoing, 'ep', split_axis=0, concat_axis=0, tiled=True)  76.8 us
    all_to_all x1, blocking collectives, per_device(): lax.all_to_all(summed, 'ep', split_axis=0, concat_axis=0, tiled=True)  75 us
    dot_general x1, matrix products, per_device(): jnp.einsum('secf,efd->secd', hidden, w_down, preferred_element_type=jnp.f...  22.9 us
    dot_general x1, matrix products, per_device(): jnp.einsum('secd,edf->secf', received, w_gate, preferred_element_type=jnp...  8.55 us

commit v1 on v0

--- a/solution.py
+++ b/solution.py
@@ -1,12 +1,17 @@
+import functools
+
 import jax
 import jax.numpy as jnp
 from jax import lax
+from jax.experimental import pallas as pl
+from jax.experimental.pallas import tpu as pltpu
 from jax.sharding import PartitionSpec as P
 
 TOP_K = 6
 
 
 EPS = 1e-06
+MESH = pl.DeviceIdType.MESH
 
 
 def slot_table(route_rows, experts_all, capacity):
@@ -53,6 +58,260 @@
     return (combined * inverse_out[:, None] * final_gain[None, :]).astype(jnp.bfloat16)
 
 
+def fused_kernel(nz, tile, tokens_ref, gain_ref, routes_ref, rw_ref, wg_hbm, wu_hbm, wd_hbm, fgain_ref,
+                 out_ref, buf, wg, wu, wd, hid, part, dbuf, xbuf, zbuf, wsem,
+                 az_s, az_r, ax_s, ax_r, ad_s, ad_r, rd_s, rd_r, rx_s, rx_r, rz_s, rz_r):
+    rows, features = tokens_ref.shape
+    hidden_units = wg.shape[1]
+    experts = 4 * nz
+    chunk = 4 * rows
+    f32, bf16 = jnp.float32, jnp.bfloat16
+    me = lax.axis_index("ep")
+    core = lax.rem(me, 2)
+    x = lax.rem(lax.div(me, 2), 2)
+    z = lax.div(me, 4)
+    d_peer = me + 1 - 2 * core
+    x_peer = me + 2 - 4 * x
+
+    def z_of(dz):
+        return lax.rem(z + dz, nz)
+
+    def z_peer(dz):
+        return z_of(dz) * 4 + x * 2 + core
+
+    def weight_copy(which, j):
+        src, dst = ((wg_hbm, wg), (wu_hbm, wu), (wd_hbm, wd))[which]
+        cols = pl.ds(pl.multiple_of(j * tile, tile), tile)
+        return pltpu.make_async_copy(src.at[0, :, cols], dst.at[:, cols], wsem.at[which, j])
+
+    gu_tiles, d_tiles = hidden_units // tile, features // tile
+    for j in range(gu_tiles):
+        weight_copy(0, j).start()
+        weight_copy(1, j).start()
+    for j in range(d_tiles):
+        weight_copy(2, j).start()
+
+    barrier = pltpu.get_barrier_semaphore()
+    peers = [d_peer, x_peer] + [z_peer(dz) for dz in range(1, nz)]
+    for peer in peers:
+        pl.semaphore_signal(barrier, inc=1, device_id={"ep": peer}, device_id_type=MESH)
+
+    own = pl.ds(pl.multiple_of(me * rows, rows), rows)
+    tok = tokens_ref[...].astype(f32)
+    inverse = lax.rsqrt(jnp.mean(tok * tok, axis=1, keepdims=True) + EPS)
+    buf[own, :features] = (tok * inverse * gain_ref[...]).astype(bf16)
+    extra = buf.shape[1] - features
+    lanes = lax.broadcasted_iota(jnp.int32, (rows, extra), 1)
+    first = jnp.zeros((rows, extra), f32)
+    second = jnp.zeros((rows, extra), f32)
+    for k in range(routes_ref.shape[1]):
+        r, w = routes_ref[:, k:k + 1], rw_ref[:, k:k + 1]
+        first = first + jnp.where(lanes == r, w, 0.0)
+        second = second + jnp.where(lanes == r + experts, w, 0.0)
+    rest = second - second.astype(bf16).astype(f32)
+    buf[own, features:] = (first + rest).astype(bf16)
+
+    pl.semaphore_wait(barrier, len(peers))
+
+    def remote(src, dst, s, r, dev):
+        return pltpu.make_async_remote_copy(
+            src_ref=src, dst_ref=dst, send_sem=s, recv_sem=r, device_id={"ep": dev}, device_id_type=MESH
+        )
+
+    def block(e):
+        return buf.at[pl.ds(pl.multiple_of(e * rows, rows), rows), :]
+
+    def same_col(dz):
+        return block(z_of(nz - dz) * 4 + x * 2 + core)
+
+    def other_col(dz):
+        return block(z_of(nz - dz) * 4 + (1 - x) * 2 + core)
+
+    def ag_z(dz, arriving=False):
+        ref = same_col(dz) if arriving else block(me)
+        return remote(ref, ref, az_s.at[dz], az_r.at[dz], z_peer(dz))
+
+    def ag_x(dz, arriving=False):
+        ref = other_col(dz) if arriving else same_col(dz)
+        return remote(ref, ref, ax_s.at[dz], ax_r.at[dz], x_peer)
+
+    def ag_d(dz, j, arriving=False):
+        if arriving:
+            col = x if j == 0 else 1 - x
+            ref = block(z_of(nz - dz) * 4 + col * 2 + 1 - core)
+        else:
+            ref = same_col(dz) if j == 0 else other_col(dz)
+        return remote(ref, ref, ad_s.at[dz, j], ad_r.at[dz, j], d_peer)
+
+    def rs_block(dz, same_x, same_core):
+        col = x if same_x else 1 - x
+        lane = core if same_core else 1 - core
+        at = pl.multiple_of((col * 2 + lane) * rows, rows)
+        return part.at[dz, pl.ds(at, rows), :]
+
+    def rs_d(dz, j):
+        return remote(rs_block(dz, j == 0, False), dbuf.at[dz, j], rd_s.at[dz, j], rd_r.at[dz, j], d_peer)
+
+    def rs_x(dz):
+        return remote(rs_block(dz, False, True), xbuf.at[dz], rx_s.at[dz], rx_r.at[dz], x_peer)
+
+    def rs_z(dz):
+        return remote(rs_block(dz, True, True), zbuf.at[dz], rz_s.at[dz], rz_r.at[dz], z_peer(nz - dz))
+
+    away = [1] + ([nz - 1] if nz > 2 else []) + list(range(2, nz - 1))
+    order = away + [0]
+
+    ag_x(0).start()
+    for dz in away:
+        ag_z(dz).start()
+    ag_d(0, 0).start()
+
+    def forward_z(dz):
+        ag_z(dz, True).wait_recv()
+        ag_x(dz).start()
+        ag_d(dz, 0).start()
+
+    def forward_x(dz):
+        ag_x(dz, True).wait_recv()
+        ag_d(dz, 1).start()
+
+    def chunk_rows(dz):
+        return pl.ds(pl.multiple_of(z_of(nz - dz) * chunk, chunk), chunk)
+
+    def gate_up(dz, begin, end, wait):
+        here = chunk_rows(dz)
+
+        def body(j, carry):
+            if wait:
+                weight_copy(0, j).wait()
+                weight_copy(1, j).wait()
+            cols = pl.ds(pl.multiple_of(j * tile, tile), tile)
+            lhs = buf[here, :features]
+            g = jnp.dot(lhs, wg[:, cols], preferred_element_type=f32)
+            u = jnp.dot(lhs, wu[:, cols], preferred_element_type=f32)
+            hid[:, cols] = (g / (1.0 + jnp.exp(-g)) * u).astype(bf16)
+            return carry
+
+        lax.fori_loop(begin, end, body, 0)
+
+    def down(dz, wait):
+        ext = buf[chunk_rows(dz), features:].astype(f32)
+        lane = lax.broadcasted_iota(jnp.int32, ext.shape, 1)
+        mine = jnp.logical_or(lane == me, lane == me + experts)
+        weight = jnp.sum(jnp.where(mine, ext, 0.0), axis=1, keepdims=True)
+
+        def body(j, carry):
+            if wait:
+                weight_copy(2, j).wait()
+            cols = pl.ds(pl.multiple_of(j * tile, tile), tile)
+            o = jnp.dot(hid[...], wd[:, cols], preferred_element_type=f32)
+            part[dz, :, cols] = (o * weight).astype(bf16)
+            return carry
+
+        lax.fori_loop(0, d_tiles, body, 0)
+
+    def finish_d(dz):
+        rs_d(dz, 1).wait_recv()
+        ref = rs_block(dz, False, True)
+        ref[...] = (ref[...].astype(f32) + dbuf[dz, 1].astype(f32)).astype(bf16)
+        rs_d(dz, 0).wait_recv()
+        rs_x(dz).start()
+
+    def finish_x(dz):
+        rs_x(dz).wait_recv()
+        ref = rs_block(dz, True, True)
+        total = ref[...].astype(f32) + dbuf[dz, 0].astype(f32) + xbuf[dz].astype(f32)
+        if dz == 0:
+            return total
+        ref[...] = total.astype(bf16)
+        return None
+
+    for dz in away:
+        forward_z(dz)
+    forward_x(0)
+    forward_x(order[0])
+
+    half = max(1, gu_tiles // 2)
+    for i, dz in enumerate(order):
+        if dz == 0:
+            ag_d(0, 0, True).wait_recv()
+            ag_d(0, 1, True).wait_recv()
+        else:
+            ag_d(dz, 0, True).wait_recv()
+            ag_d(dz, 1, True).wait_recv()
+        gate_up(dz, 0, half, i == 0)
+        if i >= 1:
+            finish_d(order[i - 1])
+        gate_up(dz, half, gu_tiles, i == 0)
+        if i + 1 < len(order) and order[i + 1] != 0:
+            forward_x(order[i + 1])
+        if i >= 2:
+            finish_x(order[i - 2])
+        down(dz, i == 0)
+        if i >= 2:
+            rs_z(order[i - 2]).start()
+        rs_d(dz, 1).start()
+        rs_d(dz, 0).start()
+
+    if len(order) >= 2:
+        finish_x(order[-2])
+    finish_d(0)
+    if len(order) >= 2:
+        rs_z(order[-2]).start()
+    total = finish_x(0)
+    for dz in away:
+        rs_z(dz).wait_recv()
+        total = total + zbuf[dz].astype(f32)
+    inverse_out = lax.rsqrt(jnp.mean(total * total, axis=1, keepdims=True) + EPS)
+    out_ref[...] = (total * inverse_out * fgain_ref[...]).astype(out_ref.dtype)
+
+    for dz in order:
+        ag_x(dz).wait_send()
+        rs_x(dz).wait_send()
+        for j in range(2):
+            ag_d(dz, j).wait_send()
+            rs_d(dz, j).wait_send()
+        if dz:
+            ag_z(dz).wait_send()
+            rs_z(dz).wait_send()
+
+
+def fused_device(tokens, norm_gain, routes, route_weights, w_gate, w_up, w_down, final_gain):
+    rows, features = tokens.shape
+    hidden_units = w_gate.shape[2]
+    experts = lax.axis_size("ep")
+    nz = experts // 4
+    tile = 512
+    extra = -(-2 * experts // 128) * 128
+    vmem, anywhere = pl.BlockSpec(memory_space=pltpu.VMEM), pl.BlockSpec(memory_space=pl.ANY)
+    dma = pltpu.SemaphoreType.DMA
+    bf16 = jnp.bfloat16
+    tiles = max(hidden_units, features) // tile
+    return pl.pallas_call(
+        functools.partial(fused_kernel, nz, tile),
+        out_shape=jax.ShapeDtypeStruct((rows, features), jnp.bfloat16),
+        in_specs=[vmem, vmem, vmem, vmem, anywhere, anywhere, anywhere, vmem],
+        out_specs=vmem,
+        scratch_shapes=[
+            pltpu.VMEM((experts * rows, features + extra), bf16),
+            pltpu.VMEM((features, hidden_units), bf16),
+            pltpu.VMEM((features, hidden_units), bf16),
+            pltpu.VMEM((hidden_units, features), bf16),
+            pltpu.VMEM((4 * rows, hidden_units), bf16),
+            pltpu.VMEM((nz, 4 * rows, features), bf16),
+            pltpu.VMEM((nz, 2, rows, features), bf16),
+            pltpu.VMEM((nz, rows, features), bf16),
+            pltpu.VMEM((nz, rows, features), bf16),
+            dma((3, tiles)),
+            dma((nz,)), dma((nz,)), dma((nz,)), dma((nz,)), dma((nz, 2)), dma((nz, 2)),
+            dma((nz, 2)), dma((nz, 2)), dma((nz,)), dma((nz,)), dma((nz,)), dma((nz,)),
+        ],
+        compiler_params=pltpu.CompilerParams(
+            collective_id=0, has_side_effects=True, vmem_limit_bytes=60 * 1024 * 1024
+        ),
+    )(tokens, norm_gain[None, :], routes, route_weights, w_gate, w_up, w_down, final_gain[None, :])
+
+
 def solution(mesh):
     placed = (
         P(("grp", "ep"), None),
@@ -64,6 +323,17 @@
         P("ep", "tp", None),
         P("tp"),
     )
+    ep, tp = mesh.shape["ep"], mesh.shape["tp"]
+
+    def step(*args):
+        rows, features = args[0].shape
+        hidden_units = args[4].shape[2]
+        fits = 3 * features * hidden_units + 3 * ep * rows * features < 24 * 2 ** 20
+        whole_tiles = features % 512 == 0 and hidden_units % 512 == 0 and rows % 16 == 0
+        if tp == 1 and ep % 4 == 0 and ep > 4 and args[4].shape[0] == 1 and fits and whole_tiles:
+            return fused_device(*args)
+        return per_device(*args)
+
     return jax.shard_map(
-        per_device, mesh=mesh, in_specs=placed, out_specs=P(("grp", "ep"), "tp"), check_vma=False
+        step, mesh=mesh, in_specs=placed, out_specs=P(("grp", "ep"), "tp"), check_vma=False
     )

time: 195 us -> 92.1 us (0.47)
  blocking collectives: 152 us -> 0 us
  Pallas kernels: 0 us -> 87.4 us
  matrix products: 35.7 us -> 0 us
  other arithmetic: 4.93 us -> 0 us
  local copies, waits for them, and re-layouts: 1.48 us -> 4.43 us
    all_to_all x2 -> x0, blocking collectives: 152 us -> none  [the longest x1 76.8 us: per_device(): lax.all_to_all(outgoing, 'ep', split_axis=0, concat_axis=0, tiled=True)]
    pallas_call x0 -> x1, Pallas kernels: none -> 87.4 us  [fused_device(): pl.pallas_call(functools.partial(fused_kernel, nz, tile), out_shape=jax.S...]
    dot_general x4 -> x0, matrix products: 35.7 us -> none  [the longest x1 22.9 us: per_device(): jnp.einsum('secf,efd->secd', hidden, w_down, preferred_element_type=jnp.f...]
    unnamed x5 -> x3, local copies, waits for them, and re-layouts: 0.78 us -> 4.43 us
    reduce_sum x3 -> x0, other arithmetic: 2.32 us -> none  [the longest x1 1.12 us: per_device(): jnp.sum(matched.astype(jnp.float32), axis=1).T.astype(jnp.bfloat16)]
where the time goes in v1:
time: 92.1 us; the launch traced here: 91.8 us
  Pallas kernels  87.4 us (95%)
  local copies, waits for them, and re-layouts  4.43 us (5%)
    pallas_call x1, Pallas kernels, fused_device(): pl.pallas_call(functools.partial(fused_kernel, nz, tile), out_shape=jax.S...  87.4 us
    unnamed x3, local copies, waits for them, and re-layouts  4.43 us

profile of v1, /device:TPU:0, one launch (start us, length us, event | category | flops | bytes accessed | tf_op | source)
XLA Modules:
  0.0 91.8 jit_solution(7850088467152326316)
XLA Ops:
  0.0 1.4 %copy.9.routes_ref = s32[64,6]{1,0:T(8,128)} copy(s32[64,6]{0,1:T(8,128)} %param.10) | data formatting | bytes 3072 | tf_op args[2]
  1.4 1.4 %copy.10.rw_ref = f32[64,6]{1,0:T(8,128)} copy(f32[64,6]{0,1:T(8,128)} %param.11) | data formatting | bytes 3072 | tf_op args[3]
  2.8 87.4 %shard_map.82 = bf16[64,2048]{1,0:T(8,128)(2,1)} custom-call(bf16[64,2048]{1,0:T(8,128)(2,1)} %tokens_ref.1, f32[1,2048]{1,0:T(1,128)} %bitcast.2, s32[64,6]{1,0:T(8,128)} %copy.9.routes_ref, f32[64,6]{1,0:T(8,128)} %copy.10.rw_ref, bf16[1,2048,2048]{2,1,0:T(8,128)(2,1)} %wg_hbm.1, bf16[1,2048,2048]{2,1,0:T(8,128)(2,1)} %wu_hbm.1, ...), custom_call_target="tpu_custom_call" | custom-call | tf_op jit(solution)/shard_map/pallas_call | solution.py:290
  90.2 1.7 %copy.12 = bf16[64,2048]{1,0:T(8,128)(2,1)} copy(bf16[64,2048]{1,0:T(8,128)(2,1)} %shard_map.82) | data formatting | bytes 524288

commit v2 on v1

--- a/solution.py
+++ b/solution.py
@@ -121,65 +121,90 @@
     def block(e):
         return buf.at[pl.ds(pl.multiple_of(e * rows, rows), rows), :]
 
-    def same_col(dz):
-        return block(z_of(nz - dz) * 4 + x * 2 + core)
-
-    def other_col(dz):
-        return block(z_of(nz - dz) * 4 + (1 - x) * 2 + core)
-
-    def ag_z(dz, arriving=False):
-        ref = same_col(dz) if arriving else block(me)
-        return remote(ref, ref, az_s.at[dz], az_r.at[dz], z_peer(dz))
-
-    def ag_x(dz, arriving=False):
-        ref = other_col(dz) if arriving else same_col(dz)
-        return remote(ref, ref, ax_s.at[dz], ax_r.at[dz], x_peer)
-
-    def ag_d(dz, j, arriving=False):
+    own_step = nz - 1
+    tables = [sorted((p for p in range(nz) if p != q), key=lambda p: (abs(p - q), p)) for q in range(nz)]
+    places = []
+    for i in range(own_step):
+        value = tables[0][i]
+        for q in range(1, nz):
+            value = jnp.where(z == q, tables[q][i], value)
+        places.append(value)
+    places.append(z)
+
+    def same_col(i):
+        return block(places[i] * 4 + x * 2 + core)
+
+    def other_col(i):
+        return block(places[i] * 4 + (1 - x) * 2 + core)
+
+    def ag_z(i, up):
+        ref = same_col(i)
+        peer = me + 4 if up else me - 4
+        return remote(ref, ref, az_s.at[i, int(up)], az_r.at[places[i]], peer)
+
+    def ag_x(i, arriving=False):
+        ref = other_col(i) if arriving else same_col(i)
+        return remote(ref, ref, ax_s.at[i], ax_r.at[i], x_peer)
+
+    def ag_d(i, j, arriving=False):
         if arriving:
             col = x if j == 0 else 1 - x
-            ref = block(z_of(nz - dz) * 4 + col * 2 + 1 - core)
+            ref = block(places[i] * 4 + col * 2 + 1 - core)
         else:
-            ref = same_col(dz) if j == 0 else other_col(dz)
-        return remote(ref, ref, ad_s.at[dz, j], ad_r.at[dz, j], d_peer)
-
-    def rs_block(dz, same_x, same_core):
+            ref = same_col(i) if j == 0 else other_col(i)
+        return remote(ref, ref, ad_s.at[i, j], ad_r.at[i, j], d_peer)
+
+    def rs_block(i, same_x, same_core):
         col = x if same_x else 1 - x
         lane = core if same_core else 1 - core
         at = pl.multiple_of((col * 2 + lane) * rows, rows)
-        return part.at[dz, pl.ds(at, rows), :]
-
-    def rs_d(dz, j):
-        return remote(rs_block(dz, j == 0, False), dbuf.at[dz, j], rd_s.at[dz, j], rd_r.at[dz, j], d_peer)
-
-    def rs_x(dz):
-        return remote(rs_block(dz, False, True), xbuf.at[dz], rx_s.at[dz], rx_r.at[dz], x_peer)
-
-    def rs_z(dz):
-        return remote(rs_block(dz, True, True), zbuf.at[dz], rz_s.at[dz], rz_r.at[dz], z_peer(nz - dz))
-
-    away = [1] + ([nz - 1] if nz > 2 else []) + list(range(2, nz - 1))
-    order = away + [0]
-
-    ag_x(0).start()
-    for dz in away:
-        ag_z(dz).start()
-    ag_d(0, 0).start()
-
-    def forward_z(dz):
-        ag_z(dz, True).wait_recv()
-        ag_x(dz).start()
-        ag_d(dz, 0).start()
-
-    def forward_x(dz):
-        ag_x(dz, True).wait_recv()
-        ag_d(dz, 1).start()
-
-    def chunk_rows(dz):
-        return pl.ds(pl.multiple_of(z_of(nz - dz) * chunk, chunk), chunk)
-
-    def gate_up(dz, begin, end, wait):
-        here = chunk_rows(dz)
+        return part.at[i, pl.ds(at, rows), :]
+
+    def rs_d(i, j):
+        return remote(rs_block(i, j == 0, False), dbuf.at[i, j], rd_s.at[i, j], rd_r.at[i, j], d_peer)
+
+    def rs_x(i):
+        return remote(rs_block(i, False, True), xbuf.at[i], rx_s.at[i], rx_r.at[i], x_peer)
+
+    def rs_z(i):
+        peer = places[i] * 4 + x * 2 + core
+        return remote(rs_block(i, True, True), zbuf.at[z], rz_s.at[i], rz_r.at[z], peer)
+
+    def rs_z_arriving(i):
+        peer = places[i] * 4 + x * 2 + core
+        ref = zbuf.at[places[i]]
+        return remote(ref, ref, rz_s.at[i], rz_r.at[places[i]], peer)
+
+    def pass_on(i, action):
+        from_below, from_above = places[i] <= z, places[i] >= z
+
+        @pl.when(jnp.logical_and(from_below, z < nz - 1))
+        def _():
+            action(ag_z(i, True))
+
+        @pl.when(jnp.logical_and(from_above, z > 0))
+        def _():
+            action(ag_z(i, False))
+
+    pass_on(own_step, lambda copy: copy.start())
+    ag_x(own_step).start()
+    ag_d(own_step, 0).start()
+
+    def forward_z(i):
+        ag_z(i, True).wait_recv()
+        pass_on(i, lambda copy: copy.start())
+        ag_x(i).start()
+        ag_d(i, 0).start()
+
+    def forward_x(i):
+        ag_x(i, True).wait_recv()
+        ag_d(i, 1).start()
+
+    def chunk_rows(i):
+        return pl.ds(pl.multiple_of(places[i] * chunk, chunk), chunk)
+
+    def gate_up(i, begin, end, wait):
+        here = chunk_rows(i)
 
         def body(j, carry):
             if wait:
@@ -194,8 +219,8 @@
 
         lax.fori_loop(begin, end, body, 0)
 
-    def down(dz, wait):
-        ext = buf[chunk_rows(dz), features:].astype(f32)
+    def down(i, begin, end, wait):
+        ext = buf[chunk_rows(i), features:].astype(f32)
         lane = lax.broadcasted_iota(jnp.int32, ext.shape, 1)
         mine = jnp.logical_or(lane == me, lane == me + experts)
         weight = jnp.sum(jnp.where(mine, ext, 0.0), axis=1, keepdims=True)
@@ -205,75 +230,70 @@
                 weight_copy(2, j).wait()
             cols = pl.ds(pl.multiple_of(j * tile, tile), tile)
             o = jnp.dot(hid[...], wd[:, cols], preferred_element_type=f32)
-            part[dz, :, cols] = (o * weight).astype(bf16)
+            part[i, :, cols] = (o * weight).astype(bf16)
             return carry
 
-        lax.fori_loop(0, d_tiles, body, 0)
-
-    def finish_d(dz):
-        rs_d(dz, 1).wait_recv()
-        ref = rs_block(dz, False, True)
-        ref[...] = (ref[...].astype(f32) + dbuf[dz, 1].astype(f32)).astype(bf16)
-        rs_d(dz, 0).wait_recv()
-        rs_x(dz).start()
-
-    def finish_x(dz):
-        rs_x(dz).wait_recv()
-        ref = rs_block(dz, True, True)
-        total = ref[...].astype(f32) + dbuf[dz, 0].astype(f32) + xbuf[dz].astype(f32)
-        if dz == 0:
+        lax.fori_loop(begin, end, body, 0)
+
+    def finish_d(i):
+        rs_d(i, 1).wait_recv()
+        ref = rs_block(i, False, True)
+        ref[...] = (ref[...].astype(f32) + dbuf[i, 1].astype(f32)).astype(bf16)
+        rs_d(i, 0).wait_recv()
+        rs_x(i).start()
+
+    def finish_x(i):
+        rs_x(i).wait_recv()
+        ref = rs_block(i, True, True)
+        total = ref[...].astype(f32) + dbuf[i, 0].astype(f32) + xbuf[i].astype(f32)
+        if i == own_step:
             return total
         ref[...] = total.astype(bf16)
+        rs_z(i).start()
         return None
 
-    for dz in away:
-        forward_z(dz)
+    forward_z(0)
+    forward_x(own_step)
+    forward_z(1)
     forward_x(0)
-    forward_x(order[0])
-
-    half = max(1, gu_tiles // 2)
-    for i, dz in enumerate(order):
-        if dz == 0:
-            ag_d(0, 0, True).wait_recv()
-            ag_d(0, 1, True).wait_recv()
-        else:
-            ag_d(dz, 0, True).wait_recv()
-            ag_d(dz, 1, True).wait_recv()
-        gate_up(dz, 0, half, i == 0)
+
+    gu_half, d_half = max(1, gu_tiles // 2), max(1, d_tiles // 2)
+    for i in range(nz):
+        ag_d(i, 0, True).wait_recv()
+        ag_d(i, 1, True).wait_recv()
+        gate_up(i, 0, gu_half, i == 0)
         if i >= 1:
-            finish_d(order[i - 1])
-        gate_up(dz, half, gu_tiles, i == 0)
-        if i + 1 < len(order) and order[i + 1] != 0:
-            forward_x(order[i + 1])
+            finish_d(i - 1)
+        gate_up(i, gu_half, gu_tiles, i == 0)
+        down(i, 0, d_half, i == 0)
+        if i + 1 < own_step:
+            forward_x(i + 1)
         if i >= 2:
-            finish_x(order[i - 2])
-        down(dz, i == 0)
-        if i >= 2:
-            rs_z(order[i - 2]).start()
-        rs_d(dz, 1).start()
-        rs_d(dz, 0).start()
-
-    if len(order) >= 2:
-        finish_x(order[-2])
-    finish_d(0)
-    if len(order) >= 2:
-        rs_z(order[-2]).start()
-    total = finish_x(0)
-    for dz in away:
-        rs_z(dz).wait_recv()
-        total = total + zbuf[dz].astype(f32)
+            finish_x(i - 2)
+        down(i, d_half, d_tiles, i == 0)
+        rs_d(i, 1).start()
+        rs_d(i, 0).start()
+        if i + 2 < own_step:
+            forward_z(i + 2)
+
+    finish_d(own_step)
+    finish_x(own_step - 1)
+    total = finish_x(own_step)
+    for i in range(own_step):
+        rs_z_arriving(i).wait_recv()
+        total = total + zbuf[places[i]].astype(f32)
     inverse_out = lax.rsqrt(jnp.mean(total * total, axis=1, keepdims=True) + EPS)
     out_ref[...] = (total * inverse_out * fgain_ref[...]).astype(out_ref.dtype)
 
-    for dz in order:
-        ag_x(dz).wait_send()
-        rs_x(dz).wait_send()
+    for i in range(nz):
+        pass_on(i, lambda copy: copy.wait_send())
+        ag_x(i).wait_send()
+        rs_x(i).wait_send()
         for j in range(2):
-            ag_d(dz, j).wait_send()
-            rs_d(dz, j).wait_send()
-        if dz:
-            ag_z(dz).wait_send()
-            rs_z(dz).wait_send()
+            ag_d(i, j).wait_send()
+            rs_d(i, j).wait_send()
+        if i < own_step:
+            rs_z(i).wait_send()
 
 
 def fused_device(tokens, norm_gain, routes, route_weights, w_gate, w_up, w_down, final_gain):
@@ -281,7 +301,7 @@
     hidden_units = w_gate.shape[2]
     experts = lax.axis_size("ep")
     nz = experts // 4
-    tile = 512
+    tile = 1024
     extra = -(-2 * experts // 128) * 128
     vmem, anywhere = pl.BlockSpec(memory_space=pltpu.VMEM), pl.BlockSpec(memory_space=pl.ANY)
     dma = pltpu.SemaphoreType.DMA
@@ -303,7 +323,7 @@
             pltpu.VMEM((nz, rows, features), bf16),
             pltpu.VMEM((nz, rows, features), bf16),
             dma((3, tiles)),
-            dma((nz,)), dma((nz,)), dma((nz,)), dma((nz,)), dma((nz, 2)), dma((nz, 2)),
+            dma((nz, 2)), dma((nz,)), dma((nz,)), dma((nz,)), dma((nz, 2)), dma((nz, 2)),
             dma((nz, 2)), dma((nz, 2)), dma((nz,)), dma((nz,)), dma((nz,)), dma((nz,)),
         ],
         compiler_params=pltpu.CompilerParams(
@@ -329,8 +349,8 @@
         rows, features = args[0].shape
         hidden_units = args[4].shape[2]
         fits = 3 * features * hidden_units + 3 * ep * rows * features < 24 * 2 ** 20
-        whole_tiles = features % 512 == 0 and hidden_units % 512 == 0 and rows % 16 == 0
-        if tp == 1 and ep % 4 == 0 and ep > 4 and args[4].shape[0] == 1 and fits and whole_tiles:
+        whole_tiles = features % 1024 == 0 and hidden_units % 1024 == 0 and rows % 16 == 0
+        if tp == 1 and ep % 4 == 0 and ep >= 12 and args[4].shape[0] == 1 and fits and whole_tiles:
             return fused_device(*args)
         return per_device(*args)
 

time: 92.1 us -> 82.7 us (0.90)
  Pallas kernels: 87.4 us -> 78 us
    pallas_call x1, Pallas kernels: 87.4 us -> 78 us  [fused_device(): pl.pallas_call(functools.partial(fused_kernel, nz, tile), out_shape=jax.S...]
where the time goes in v2:
time: 82.7 us; the launch traced here: 82.5 us
  Pallas kernels  78 us (94%)
  local copies, waits for them, and re-layouts  4.43 us (5%)
    pallas_call x1, Pallas kernels, fused_device(): pl.pallas_call(functools.partial(fused_kernel, nz, tile), out_shape=jax.S...  78 us
    unnamed x3, local copies, waits for them, and re-layouts  4.43 us

profile of v2, /device:TPU:0, one launch (start us, length us, event | category | flops | bytes accessed | tf_op | source)
XLA Modules:
  0.0 82.5 jit_solution(8758753401535222895)
XLA Ops:
  0.0 1.4 %copy.9.routes_ref = s32[64,6]{1,0:T(8,128)} copy(s32[64,6]{0,1:T(8,128)} %param.10) | data formatting | bytes 3072 | tf_op args[2]
  1.4 1.4 %copy.10.rw_ref = f32[64,6]{1,0:T(8,128)} copy(f32[64,6]{0,1:T(8,128)} %param.11) | data formatting | bytes 3072 | tf_op args[3]
  2.8 78.0 %shard_map.82 = bf16[64,2048]{1,0:T(8,128)(2,1)} custom-call(bf16[64,2048]{1,0:T(8,128)(2,1)} %tokens_ref.1, f32[1,2048]{1,0:T(1,128)} %bitcast.2, s32[64,6]{1,0:T(8,128)} %copy.9.routes_ref, f32[64,6]{1,0:T(8,128)} %copy.10.rw_ref, bf16[1,2048,2048]{2,1,0:T(8,128)(2,1)} %wg_hbm.1, bf16[1,2048,2048]{2,1,0:T(8,128)(2,1)} %wu_hbm.1, ...), custom_call_target="tpu_custom_call" | custom-call | tf_op jit(solution)/shard_map/pallas_call | solution.py:310
  80.8 1.7 %copy.12 = bf16[64,2048]{1,0:T(8,128)(2,1)} copy(bf16[64,2048]{1,0:T(8,128)(2,1)} %shard_map.82) | data formatting | bytes 524288
